TPU v7x, 32 devices: a whole 2x2x4 slice. The times are simulated.
32 devices in a mesh: ep: 8 (over z, x), tp: 4 (over y, core).
Axes of the slice: x: 2, y: 2, z: 4, core: 2. Of those that a mesh axis runs over, the one named last changes fastest.
Arguments:
- queries: bfloat16 [1024, 4096], P('ep', 'tp'), may hold values from -112 to 112
- key_rows: bfloat16 [1024, 4096], P('ep', 'tp'), may hold values from -8.1 to 8.1
- values: bfloat16 [1024, 4096], P('ep', 'tp'), may hold values from -6 to 6
- lambdas: float32 [16], P('tp'), may hold values from 0.3 to 0.8
- head_gain: float32 [256], replicated, may hold values from 0.1 to 1.9
- tokens: bfloat16 [512, 4096], P('ep'), may hold values from -6 to 6
- moe_gain: float32 [4096], replicated, may hold values from 0.1 to 1.9
- routes: int32 [512, 2], P('ep'), may hold values from 0 to 7, all different within a row; in each aligned block of 64 rows (0 to 63, 64 to 127, ...) at most 32 rows name the same one
- route_scores: float32 [512, 2], P('ep'), may hold values from -6 to 6
- w_gate: bfloat16 [8, 4096, 2048], P('ep', None, 'tp'), may hold values from -0.09375 to 0.09375
- w_up: bfloat16 [8, 4096, 2048], P('ep', None, 'tp'), may hold values from -0.09375 to 0.09375
- w_down: bfloat16 [8, 2048, 4096], P('ep', 'tp'), may hold values from -0.125 to 0.125
Outputs:
- attended: bfloat16 [1024, 4096], P('ep', 'tp')
- expert_out: bfloat16 [512, 4096], P('ep', 'tp')
Inputs may be any that keep to these rules, and one draw needn't show every extreme that they name: `routes`: each row names 2 different experts. Among the rows of one index of ep at most 32 name the same expert, and some index reaches 32 in every draw.
All inputs are finite; a program needn't handle non-finite values.
Results may differ from a plain program's by a relative error of at most 0.018.
Values may be sent and summed in bfloat16 or wider, within the bound.
A program may use at most 64 MiB of HBM per device.

v0:
```python
import jax
import jax.numpy as jnp
from jax import lax
from jax.sharding import PartitionSpec as P

QKD = 128
VD = 256
TOP = 2
neg_big = -1e30
head_eps = 1e-05
moe_eps = 1e-06
head_scale = 0.8


def slot_table(routes, experts, capacity):
    flat_routes = routes.reshape(-1)
    onehot = (flat_routes[:, None] == jnp.arange(experts, dtype=jnp.int32)[None, :]).astype(
        jnp.int32
    )
    before = jnp.cumsum(onehot, axis=0) - onehot
    position = jnp.sum(before * onehot, axis=1)
    return (flat_routes * capacity + position).reshape(routes.shape)


def fold_block(state, query_group, query_pos, key_heads, value_heads, key_pos):
    maxima, denominators, accumulated = state
    scores = jnp.einsum(
        "qhmd,khmd->hmqk", query_group, key_heads, preferred_element_type=jnp.float32
    ) * QKD ** (-0.5)
    visible = key_pos[None, :] <= query_pos[:, None]
    scores = jnp.where(visible, scores, neg_big)
    new_max = jnp.maximum(maxima, jnp.max(scores, axis=-1))
    weights = jnp.where(visible, jnp.exp(scores - new_max[..., None]), 0.0)
    accumulated = jnp.einsum(
        "hmqk,khd->hmqd", weights, value_heads, precision=lax.Precision.HIGHEST
    )
    denominators = jnp.sum(weights, axis=-1)
    return (new_max, denominators, accumulated)


def local(
    queries,
    key_rows,
    values,
    lambdas,
    head_gain,
    tokens,
    moe_gain,
    routes,
    route_scores,
    w_gate,
    w_up,
    w_down,
):
    rows_a = queries.shape[0]
    half_rows = rows_a // 2
    head_local = lambdas.shape[0]
    ep_count = lax.axis_size("ep")
    ep_index = lax.axis_index("ep")
    early_queries = queries[:half_rows]
    later_queries = queries[half_rows:]
    early_pos = ep_index * rows_a + jnp.arange(half_rows, dtype=jnp.int32)
    later_pos = ep_index * rows_a + half_rows + jnp.arange(half_rows, dtype=jnp.int32)
    query_groups = (
        early_queries.reshape(half_rows, head_local, 2, QKD),
        later_queries.reshape(half_rows, head_local, 2, QKD),
    )
    position_groups = (early_pos, later_pos)
    start_state = (
        jnp.full((head_local, 2, half_rows), neg_big, jnp.float32),
        jnp.zeros((head_local, 2, half_rows), jnp.float32),
        jnp.zeros((head_local, 2, half_rows, VD), jnp.float32),
    )
    totals = (start_state, start_state)
    row_start = jnp.int32(0)
    key_block = lax.all_gather(key_rows, "ep", axis=0, tiled=True)
    value_block = lax.all_gather(values, "ep", axis=0, tiled=True)
    key_count = key_block.shape[0]
    key_heads = key_block.reshape(key_count, head_local, 2, QKD)
    value_heads = value_block.reshape(key_count, head_local, VD).astype(jnp.float32)
    key_pos = jnp.arange(key_count, dtype=jnp.int32)
    updated = []
    for attend_group_index in range(2):
        state = totals[attend_group_index]
        query_group = query_groups[attend_group_index]
        query_pos = position_groups[attend_group_index]
        state = lax.cond(
            row_start <= query_pos[-1],
            lambda held: fold_block(held, query_group, query_pos, key_heads, value_heads, key_pos),
            lambda held: held,
            state,
        )
        updated.append(state)
    folded = (updated[0], updated[1])
    attended_groups = []
    for group_index in range(2):
        maxima, denominators, accumulated = folded[group_index]
        mixed_out = (
            accumulated[:, 0] / denominators[:, 0, :, None]
            - lambdas[:, None, None] * accumulated[:, 1] / denominators[:, 1, :, None]
        )
        scaled = mixed_out * lax.rsqrt(
            jnp.mean(mixed_out * mixed_out, axis=-1, keepdims=True) + head_eps
        )
        scaled = scaled * head_gain * head_scale
        attended_groups.append(
            scaled.transpose(1, 0, 2).reshape(half_rows, head_local * VD).astype(jnp.bfloat16)
        )
    later_out = attended_groups[1]
    attended = jnp.concatenate([attended_groups[0], later_out], axis=0)
    rows_b = tokens.shape[0]
    capacity = 2 * TOP * rows_b // ep_count
    token_f32 = tokens.astype(jnp.float32)
    normed = (
        token_f32
        * lax.rsqrt(jnp.mean(token_f32 * token_f32, axis=-1, keepdims=True) + moe_eps)
        * moe_gain
    ).astype(jnp.bfloat16)
    gate_weights = jax.nn.softmax(route_scores, axis=-1)
    slot_of = slot_table(routes, ep_count, capacity)
    row_ids = jnp.broadcast_to(jnp.arange(rows_b, dtype=jnp.int32)[:, None], slot_of.shape)
    row_of_slot = (
        jnp.zeros((ep_count * capacity,), jnp.int32)
        .at[slot_of.reshape(-1)]
        .set(row_ids.reshape(-1))
    )
    gate_local = w_gate[0]
    up_local = w_up[0]
    down_local = w_down[0]
    outgoing = normed[row_of_slot]
    arrived = lax.all_to_all(outgoing, "ep", split_axis=0, concat_axis=0, tiled=True)
    gate_act = jnp.dot(arrived, gate_local, preferred_element_type=jnp.float32)
    up_act = jnp.dot(arrived, up_local, preferred_element_type=jnp.float32)
    hidden = (jax.nn.silu(gate_act) * up_act).astype(jnp.bfloat16)
    summed = lax.psum_scatter(
        lax.dot_general(
            down_local, hidden, (((0,), (1,)), ((), ())), preferred_element_type=jnp.float32
        ).astype(jnp.bfloat16),
        "tp",
        scatter_dimension=0,
        tiled=True,
    )
    returned = lax.all_to_all(summed, "ep", split_axis=1, concat_axis=1, tiled=True)
    slot_ids = jnp.arange(ep_count * capacity, dtype=jnp.int32)
    combined = jnp.zeros((rows_b, returned.shape[0]), jnp.float32)
    for choice_index in range(TOP):
        picker = (slot_of[:, choice_index, None] == slot_ids[None, :]).astype(jnp.bfloat16)
        picked = lax.dot_general(
            picker, returned, (((1,), (1,)), ((), ())), preferred_element_type=jnp.float32
        )
        combined = combined + gate_weights[:, choice_index, None] * picked
    expert_out = combined.astype(jnp.bfloat16)
    return (attended, expert_out)


def solution(mesh):
    return jax.shard_map(
        local,
        mesh=mesh,
        in_specs=(
            P("ep", "tp"),
            P("ep", "tp"),
            P("ep", "tp"),
            P("tp"),
            P(),
            P("ep", None),
            P(),
            P("ep", None),
            P("ep", None),
            P("ep", None, "tp"),
            P("ep", None, "tp"),
            P("ep", "tp", None),
        ),
        out_specs=(P("ep", "tp"), P("ep", "tp")),
        check_vma=False,
    )
```

profile of v0, /device:TPU:0, one launch (start us, length us, event | category | flops | bytes accessed | tf_op | source)
XLA Modules:
  0.0 190.7 jit_solution(13893074613434656306)
XLA Ops:
  8.1 1.9 copy.24
  9.9 0.8 copy.34
  11.8 1.0 scatter_custom_fusion
  12.8 1.2 fusion.42
  14.0 0.9 fusion.44
  15.0 3.2 %gather_fusion = bf16[256,4096]{1,0:T(8,128)(2,1)} fusion(bf16[64,4096]{1,0:T(8,128)(2,1)S(1)} %fusion.44, s32[1024]{0:T(1024)S(1)} %pad_clamp_fusion), kind=kCustom, calls=%fused_computation | custom fusion | bytes 4195328 | tf_op jit(solution)/shard_map/gather | solution.py:130
  18.2 7.4 %all-to-all-start = ((bf16[8,32,4096]{2,1,0:T(8,128)(2,1)}), bf16[8,32,4096]{2,1,0:T(8,128)(2,1)S(1)}, u32[]{:S(2)}, u32[]{:S(2)}) async-start(bf16[8,32,4096]{2,1,0:T(8,128)(2,1)} %bitcast.20), calls=%async_computation | async-start | bytes 4194304 | tf_op jit(solution)/shard_map/all_to_all | solution.py:131
  25.6 0.8 copy.23
  26.5 69.8 %all-to-all-done = bf16[8,32,4096]{2,1,0:T(8,128)(2,1)S(1)} async-done(((bf16[8,32,4096]{2,1,0:T(8,128)(2,1)}), bf16[8,32,4096]{2,1,0:T(8,128)(2,1)S(1)}, u32[]{:S(2)}, u32[]{:S(2)}) %all-to-all-start) | async-done | bytes 2097184 | tf_op jit(solution)/shard_map/all_to_all | solution.py:131
  96.3 3.5 %fusion.32 = f32[256,512]{1,0:T(8,128)S(1)} fusion(bf16[256,4096]{1,0:T(8,128)(2,1)S(1)} %bitcast.99, bf16[1,4096,512]{2,1,0:T(8,128)(2,1)} %param.25), kind=kOutput, calls=%fused_computation.43 | convolution fusion | flops 1073741824 | bytes 6815744 | tf_op jit(solution)/shard_map/dot_general | solution.py:132
  99.8 7.4 %fusion.28 = bf16[4096,256]{0,1:T(8,128)(2,1)} fusion(bf16[1,512,4096]{2,1,0:T(8,128)(2,1)} %param.27, bf16[256,4096]{1,0:T(8,128)(2,1)S(1)} %bitcast.100, bf16[1,4096,512]{2,1,0:T(8,128)(2,1)} %param.26, f32[256,512]{1,0:T(8,128)S(1)} %fusion.32), kind=kOutput, calls=%fused_computation.39 | convolution fusion | flops 2149318656 | bytes 13107200 | tf_op jit(solution)/shard_map/dot_general | solution.py:136
  107.2 0.6 slice.55
  108.5 0.6 slice.50
  109.8 0.2 slice_reduce_fusion
  110.0 4.1 %convert.3 = f32[1024,4,256]{0,2,1:T(8,128)} convert(bf16[1024,4,256]{0,2,1:T(8,128)(2,1)} %bitcast.98) | non-fusion elementwise | flops 1048576 | bytes 6291456 | tf_op jit(solution)/shard_map/convert_element_type | solution.py:80
  114.1 33.2 %all-gather.3.cloned.1.call-done = bf16[1024,1024]{0,1:T(8,128)(2,1)} async-done(((bf16[128,1024]{0,1:T(8,128)(2,1)}), bf16[1024,1024]{0,1:T(8,128)(2,1)}) %all-gather.3.cloned.1.call-update) | async-done | bytes 2097168 | tf_op jit(solution)/shard_map/all_gather | solution.py:76
  147.3 8.6 %conditional.3 = (f32[4,2,64]{2,1,0:T(2,128)S(1)}, f32[4,2,64,256]{3,2,1,0:T(8,128)S(1)}) conditional(s32[]{:T(128)} %bitcast.10, () %tuple.26, (s32[1024]{0:T(1024)S(1)}, s32[64]{0:T(128)S(1)}, bf16[128,1024]{1,0:T(8,128)(2,1)S(1)}, bf16[1024,4,2,128]{0,3,2,1:T(8,128)(2,1)}, f32[1024,4,256]{0,2,1:T(8,128)}) %tuple.56), branch_computations={%region_5.6_spmd, %region_6.9_spmd} | conditional | flops 1751186944 | bytes 30818604 | solution.py:87
  147.5 2.4 %fusion.16 = (f32[4,2,64]{2,1,0:T(2,128)S(1)}, f32[4,2,64,1024]{3,2,1,0:T(8,128)S(1)}) fusion(pred[64,1024]{1,0:T(8,128)(4,1)S(1)} %broadcast_compare_fusion.1, bf16[1024,4,2,128]{0,3,2,1:T(8,128)(2,1)} %get-tuple-element.52, bf16[64,4,2,128]{3,2,1,0:T(2,128)(2,1)S(1)} %reshape.109), kind=kOutput, calls=%fused_computation.24 | convolution fusion | flops 135790080 | bytes 4392960 | tf_op jit(solution)/shard_map/cond/branch_1_fun/qhmd,khmd->hmqk/dot_general | solution.py:27
  150.0 0.4 copy-done
  150.3 4.8 %fusion.14 = f32[4,2,64,256]{3,2,1,0:T(8,128)S(1)} fusion(f32[1024,4,256]{0,2,1:T(8,128)S(1)} %copy-done, f32[4,2,64,1024]{3,2,1,0:T(8,128)S(1)} %get-tuple-element.63, f32[4,2,64]{2,1,0:T(2,128)S(1)} %broadcast_maximum_fusion.1, pred[64,1024]{1,0:T(8,128)(4,1)S(1)} %broadcast_compare_fusion.1), kind=kOutput, calls=%fused_computation.20 | convolution fusion | flops 1612709888 | bytes 6883328 | tf_op jit(solution)/shard_map/cond/branch_1_fun/hmqk,khd->hmqd/dot_general | solution.py:34
  155.2 0.7 fusion.17
  155.9 8.8 %conditional.2 = (f32[4,2,64]{2,1,0:T(2,128)S(1)}, f32[4,2,64,256]{3,2,1,0:T(8,128)S(1)}) conditional(s32[]{:T(128)} %bitcast.2, () %tuple.24, (s32[1024]{0:T(1024)S(1)}, s32[64]{0:T(128)S(1)}, bf16[128,1024]{1,0:T(8,128)(2,1)S(1)}, bf16[1024,4,2,128]{0,3,2,1:T(8,128)(2,1)}, f32[1024,4,256]{0,2,1:T(8,128)}) %tuple.57), branch_computations={%region_0.0_spmd, %region_1.4_spmd} | conditional | flops 1751186944 | bytes 30818604 | solution.py:87
  156.3 2.4 %fusion.2 = (f32[4,2,64]{2,1,0:T(2,128)S(1)}, f32[4,2,64,1024]{3,2,1,0:T(8,128)S(1)}) fusion(pred[64,1024]{1,0:T(8,128)(4,1)S(1)} %broadcast_compare_fusion, bf16[1024,4,2,128]{0,3,2,1:T(8,128)(2,1)} %get-tuple-element.47, bf16[64,4,2,128]{3,2,1,0:T(2,128)(2,1)S(1)} %reshape.108), kind=kOutput, calls=%fused_computation.6 | convolution fusion | flops 135790080 | bytes 4392960 | tf_op jit(solution)/shard_map/cond/branch_1_fun/qhmd,khmd->hmqk/dot_general | solution.py:27
  158.7 0.4 copy-done.1
  159.1 4.8 %fusion = f32[4,2,64,256]{3,2,1,0:T(8,128)S(1)} fusion(f32[1024,4,256]{0,2,1:T(8,128)S(1)} %copy-done.1, f32[4,2,64,1024]{3,2,1,0:T(8,128)S(1)} %get-tuple-element.61, f32[4,2,64]{2,1,0:T(2,128)S(1)} %broadcast_maximum_fusion, pred[64,1024]{1,0:T(8,128)(4,1)S(1)} %broadcast_compare_fusion), kind=kOutput, calls=%fused_computation.2 | convolution fusion | flops 1612709888 | bytes 6883328 | tf_op jit(solution)/shard_map/cond/branch_1_fun/hmqk,khd->hmqd/dot_general | solution.py:34
  164.0 0.7 fusion.3
  164.7 3.5 %all-to-all-start.1 = ((bf16[1024,8,32]{0,2,1:T(8,128)(2,1)}), bf16[1024,8,32]{0,2,1:T(8,128)(2,1)S(1)}, u32[]{:S(2)}, u32[]{:S(2)}) async-start(bf16[1024,8,32]{0,2,1:T(8,128)(2,1)} %bitcast.101), calls=%async_computation.2 | async-start | bytes 1048576 | tf_op jit(solution)/shard_map/all_to_all | solution.py:143
  168.3 0.4 multiply_reduce_fusion.1
  168.8 0.7 pad_maximum_fusion
  169.5 12.6 %all-to-all-done.1 = bf16[1024,8,32]{0,2,1:T(8,128)(2,1)S(1)} async-done(((bf16[1024,8,32]{0,2,1:T(8,128)(2,1)}), bf16[1024,8,32]{0,2,1:T(8,128)(2,1)S(1)}, u32[]{:S(2)}, u32[]{:S(2)}) %all-to-all-start.1) | async-done | bytes 524320 | tf_op jit(solution)/shard_map/all_to_all | solution.py:143
  182.1 0.2 convolution_multiply_fusion.1
  182.4 0.9 fusion.41
  (57 shorter events, 1.9 us)
Async XLA Ops:
  8.0 6.0 %copy-start.2 = (bf16[64,4096]{1,0:T(8,128)(2,1)S(1)}, bf16[64,4096]{1,0:T(8,128)(2,1)}, u32[]{:S(2)}) copy-start(bf16[64,4096]{1,0:T(8,128)(2,1)} %param.21) | copy-start | bytes 1572868
  8.0 102.0 %all-gather.5.cloned.1.call-start = ((), (), s32[]{:S(2)}) async-start(), calls=%async_computation.4 | async-start | bytes 2359296 | tf_op jit(solution)/shard_map/all_gather | solution.py:77
  18.2 7.5 %copy-start.3 = (bf16[128,1024]{1,0:T(8,128)(2,1)S(1)}, bf16[128,1024]{1,0:T(8,128)(2,1)}, u32[]{:S(2)}) copy-start(bf16[128,1024]{1,0:T(8,128)(2,1)} %param.17) | copy-start | bytes 786436
  18.2 78.2 %all-to-all-start = ((bf16[8,32,4096]{2,1,0:T(8,128)(2,1)}), bf16[8,32,4096]{2,1,0:T(8,128)(2,1)S(1)}, u32[]{:S(2)}, u32[]{:S(2)}) async-start(bf16[8,32,4096]{2,1,0:T(8,128)(2,1)} %bitcast.20), calls=%async_computation | async-start | bytes 4194304 | tf_op jit(solution)/shard_map/all_to_all | solution.py:131
  25.6 121.7 %all-gather.3.cloned.1.call-start = ((), (), s32[]{:S(2)}) async-start(), calls=%async_computation.3 | async-start | bytes 2359296 | tf_op jit(solution)/shard_map/all_gather | solution.py:76
  26.5 138.2 %reduce-scatter.2.cloned.1.call-start = ((), (), s32[]{:S(2)}) async-start(), calls=%async_computation.5 | async-start | bytes 2621440 | tf_op jit(solution)/shard_map/reduce_scatter | solution.py:135
  107.2 2.5 %copy-start.5 = (f32[64,2]{0,1:T(2,128)S(1)}, f32[64,2]{0,1:T(2,128)}, u32[]{:S(2)}) copy-start(f32[64,2]{0,1:T(2,128)} %param.24) | copy-start | bytes 1540
  110.0 37.3 %copy-start.4 = (bf16[128,1024]{1,0:T(8,128)(2,1)S(1)}, bf16[128,1024]{1,0:T(8,128)(2,1)}, u32[]{:S(2)}) copy-start(bf16[128,1024]{1,0:T(8,128)(2,1)} %param.16) | copy-start | bytes 786436
  147.5 2.8 %copy-start = (f32[1024,4,256]{0,2,1:T(8,128)S(1)}, f32[1024,4,256]{0,2,1:T(8,128)}, u32[]{:S(2)}) copy-start(f32[1024,4,256]{0,2,1:T(8,128)} %get-tuple-element.53) | copy-start | bytes 12582916 | tf_op jit(solution)/shard_map/cond
  155.9 12.4 %copy-start.7 = (f32[4]{0:T(128)S(1)}, f32[4]{0:T(128)}, u32[]{:S(2)}) copy-start(f32[4]{0:T(128)} %param.19) | copy-start | bytes 52
  156.3 2.8 %copy-start.1 = (f32[1024,4,256]{0,2,1:T(8,128)S(1)}, f32[1024,4,256]{0,2,1:T(8,128)}, u32[]{:S(2)}) copy-start(f32[1024,4,256]{0,2,1:T(8,128)} %get-tuple-element.48) | copy-start | bytes 12582916 | tf_op jit(solution)/shard_map/cond
  164.7 4.0 %copy-start.6 = (f32[256]{0:T(256)S(1)}, f32[256]{0:T(256)}, u32[]{:S(2)}) copy-start(f32[256]{0:T(256)} %param.20) | copy-start | bytes 3076
  164.7 17.4 %all-to-all-start.1 = ((bf16[1024,8,32]{0,2,1:T(8,128)(2,1)}), bf16[1024,8,32]{0,2,1:T(8,128)(2,1)S(1)}, u32[]{:S(2)}, u32[]{:S(2)}) async-start(bf16[1024,8,32]{0,2,1:T(8,128)(2,1)} %bitcast.101), calls=%async_computation.2 | async-start | bytes 1048576 | tf_op jit(solution)/shard_map/all_to_all | solution.py:143
Sparse Core Ops, SparseCore 0:
  10.9 83.9 all-gather.4
  97.5 49.7 all-gather.2
Sparse Core Ops, SparseCore 1:
  107.3 30.1 reduce-scatter.1
where the time goes:
time: 191 us
  waiting for transfers between devices  116 us (61%)
  matrix products  26.5 us (14%)
  between operations  17.1 us (9%)
  starting transfers between devices  11 us (6%)
  local copies, waits for them, and re-layouts  10.5 us (5%)
  other arithmetic  9.63 us (5%)
    all_to_all x1, waiting for transfers between devices, local(): lax.all_to_all(outgoing, 'ep', split_axis=0, concat_axis=0, tiled=True)  69.8 us
    all_gather x1, waiting for transfers between devices, local(): key_block = lax.all_gather(key_rows, 'ep', axis=0, tiled=True)  33.2 us
    all_to_all x1, waiting for transfers between devices, local(): lax.all_to_all(summed, 'ep', split_axis=1, concat_axis=1, tiled=True)  12.6 us
    dot_general x2, matrix products, fold_block(): jnp.einsum('hmqk,khd->hmqd', weights, value_heads, precision=lax.Precisio...  9.67 us
    all_to_all x1, starting transfers between devices, local(): lax.all_to_all(outgoing, 'ep', split_axis=0, concat_axis=0, tiled=True)  7.41 us
    dot_general x1, matrix products, local(): lax.dot_general(down_local, hidden, (((0,), (1,)), ((), ())), preferred_e...  7.37 us
    dot_general x2, matrix products, fold_block(): jnp.einsum('qhmd,khmd->hmqk', query_group, key_heads, preferred_element_t...  4.85 us
    convert_element_type x1, other arithmetic, local(): value_block.reshape(key_count, head_local, VD).astype(jnp.float32)  4.08 us
  transfers between devices with their start and end apart: 5, of which 3 were waited for; matrix products, arithmetic and copies ran while one was open for 22% of the time, Pallas kernels for 0%

commit v1 on v0

--- a/solution.py
+++ b/solution.py
@@ -73,8 +73,11 @@
     )
     totals = (start_state, start_state)
     row_start = jnp.int32(0)
-    key_block = lax.all_gather(key_rows, "ep", axis=0, tiled=True)
-    value_block = lax.all_gather(values, "ep", axis=0, tiled=True)
+    key_block, value_block = jnp.split(
+        lax.all_gather(jnp.concatenate([key_rows, values], axis=1), "ep", axis=0, tiled=True),
+        [key_rows.shape[1]],
+        axis=1,
+    )
     key_count = key_block.shape[0]
     key_heads = key_block.reshape(key_count, head_local, 2, QKD)
     value_heads = value_block.reshape(key_count, head_local, VD).astype(jnp.float32)

time: 191 us -> 185 us (0.969)
  blocking collectives: 0 us -> 99.9 us
  waiting for transfers between devices: 116 us -> 18.7 us
  starting transfers between devices: 11 us -> 5.59 us
  matrix products: 26.5 us -> 21.3 us
  local copies, waits for them, and re-layouts: 10.5 us -> 14.6 us
  other arithmetic: 9.63 us -> 7.05 us
    all_to_all x0 -> x1, blocking collectives: none -> 99.9 us  [local(): lax.all_to_all(outgoing, 'ep', split_axis=0, concat_axis=0, tiled=True)]
    all_to_all x1 -> x0, waiting for transfers between devices: 69.8 us -> none  [local(): lax.all_to_all(outgoing, 'ep', split_axis=0, concat_axis=0, tiled=True)]
    all_gather x2 -> x1, waiting for transfers between devices: 33.2 us -> 0.02 us  [local(): lax.all_gather(jnp.concatenate([key_rows, values], axis=1), 'ep', axis=0,...]
    all_to_all x1 -> x0, starting transfers between devices: 7.41 us -> none  [local(): lax.all_to_all(outgoing, 'ep', split_axis=0, concat_axis=0, tiled=True)]
    reduce_scatter x1, waiting for transfers between devices: 0.03 us -> 5.68 us  [local(): lax.psum_scatter(lax.dot_general(down_local, hidden, (((0,), (1,)), ((),...]
    dot_general x2, matrix products: 4.85 us -> 1.39 us  [fold_block(): jnp.einsum('qhmd,khmd->hmqk', query_group, key_heads, preferred_element_t...]
    split x0 -> x1, local copies, waits for them, and re-layouts: none -> 3.01 us  [local(): jnp.split(lax.all_gather(jnp.concatenate([key_rows, values], axis=1), 'ep...]
    dot_general x1, matrix products: 3.5 us -> 1.24 us  [local(): gate_act = jnp.dot(arrived, gate_local, preferred_element_type=jnp.float32)]
  transfers between devices with their start and end apart: 5 -> 3, of which waited for: 3 -> 2; matrix products, arithmetic and copies ran while one was open for 22% -> 19% of each run, Pallas kernels for 0% -> 0%
where the time goes in v1:
time: 185 us; the launch traced here: 184 us
  blocking collectives  99.9 us (54%)
  matrix products  21.3 us (12%)
  waiting for transfers between devices  18.7 us (10%)
  between operations  17.1 us (9%)
  local copies, waits for them, and re-layouts  14.6 us (8%)
  other arithmetic  7.05 us (4%)
  starting transfers between devices  5.59 us (3%)
    all_to_all x1, blocking collectives, local(): lax.all_to_all(outgoing, 'ep', split_axis=0, concat_axis=0, tiled=True)  99.9 us
    all_to_all x1, waiting for transfers between devices, local(): lax.all_to_all(summed, 'ep', split_axis=1, concat_axis=1, tiled=True)  13 us
    dot_general x2, matrix products, fold_block(): jnp.einsum('hmqk,khd->hmqd', weights, value_heads, precision=lax.Precisio...  9.66 us
    dot_general x1, matrix products, local(): lax.dot_general(down_local, hidden, (((0,), (1,)), ((), ())), preferred_e...  7.85 us
    reduce_scatter x1, waiting for transfers between devices, local(): lax.psum_scatter(lax.dot_general(down_local, hidden, (((0,), (1,)), ((),...  5.68 us
    all_to_all x1, starting transfers between devices, local(): lax.all_to_all(summed, 'ep', split_axis=1, concat_axis=1, tiled=True)  5.51 us
    unnamed x21, local copies, waits for them, and re-layouts  3.76 us
  transfers between devices with their start and end apart: 3, of which 2 were waited for; matrix products, arithmetic and copies ran while one was open for 19% of the time, Pallas kernels for 0%

profile of v1, /device:TPU:0, one launch (start us, length us, event | category | flops | bytes accessed | tf_op | source)
XLA Modules:
  0.0 184.4 jit_solution(5833872621887674472)
XLA Ops:
  8.1 1.2 copy.23
  9.2 1.1 copy.24
  10.4 0.9 pad_maximum_fusion
  12.5 1.0 scatter_custom_fusion
  13.5 0.2 fusion.42
  13.7 0.2 fusion.44
  13.9 1.8 %gather_fusion = bf16[256,4096]{1,0:T(8,128)(2,1)S(1)} fusion(bf16[64,4096]{1,0:T(8,128)(2,1)S(1)} %fusion.44, s32[1024]{0:T(1024)S(1)} %pad_clamp_fusion), kind=kCustom, calls=%fused_computation | custom fusion | bytes 4195328 | tf_op jit(solution)/shard_map/gather | solution.py:133
  15.8 99.9 %all_to_all.24 = bf16[8,32,4096]{2,1,0:T(8,128)(2,1)S(1)} all-to-all(bf16[8,32,4096]{2,1,0:T(8,128)(2,1)S(1)} %bitcast.96), channel_id=1, replica_groups=mesh['ep'=8,'tp'=4] {'ep'}, dimensions={0} | all-to-all | bytes 4194304 | tf_op jit(solution)/shard_map/all_to_all | solution.py:134
  115.7 1.3 copy-done.2
  117.0 1.2 fusion.32
  118.3 7.9 %fusion.28 = bf16[4096,256]{0,1:T(8,128)(2,1)} fusion(bf16[1,512,4096]{2,1,0:T(8,128)(2,1)} %param.27, bf16[256,4096]{1,0:T(8,128)(2,1)} %bitcast.101, bf16[1,4096,512]{2,1,0:T(8,128)(2,1)} %param.26, f32[256,512]{1,0:T(8,128)S(1)} %fusion.32), kind=kOutput, calls=%fused_computation.39 | convolution fusion | flops 2149318656 | bytes 13107200 | tf_op jit(solution)/shard_map/dot_general | solution.py:139
  126.2 0.6 slice.55
  127.4 0.6 slice.50
  129.0 3.0 %fusion.74 = (bf16[1024,1024]{0,1:T(8,128)(2,1)S(1)}, bf16[1024,1024]{0,1:T(8,128)(2,1)S(1)}) fusion(bf16[1024,2048]{0,1:T(8,128)(2,1)} %all-gather.2.cloned.1.call-done), kind=kLoop, calls=%fused_computation.110 | loop fusion | bytes 8388608 | tf_op jit(solution)/shard_map/split | solution.py:76
  132.0 2.4 %convert.3 = f32[1024,4,256]{0,2,1:T(8,128)} convert(bf16[1024,4,256]{0,2,1:T(8,128)(2,1)S(1)} %bitcast.97) | non-fusion elementwise | flops 1048576 | bytes 6291456 | tf_op jit(solution)/shard_map/convert_element_type | solution.py:83
  134.4 7.9 %conditional.3 = (f32[4,2,64]{2,1,0:T(2,128)S(1)}, f32[4,2,64,256]{3,2,1,0:T(8,128)S(1)}) conditional(s32[]{:T(128)} %bitcast.10, () %tuple.26, (s32[1024]{0:T(1024)S(1)}, s32[64]{0:T(128)S(1)}, bf16[128,1024]{1,0:T(8,128)(2,1)S(1)}, bf16[1024,4,2,128]{0,3,2,1:T(8,128)(2,1)S(1)}, f32[1024,4,256]{0,2,1:T(8,128)}) %tuple.55), branch_computations={%region_5.6_spmd, %region_6.9_spmd} | conditional | flops 1751186944 | bytes 30818604 | solution.py:90
  134.6 0.7 fusion.16
  135.3 1.5 copy-done
  136.8 4.8 %fusion.14 = f32[4,2,64,256]{3,2,1,0:T(8,128)S(1)} fusion(f32[1024,4,256]{0,2,1:T(8,128)S(1)} %copy-done, f32[4,2,64,1024]{3,2,1,0:T(8,128)S(1)} %get-tuple-element.63, f32[4,2,64]{2,1,0:T(2,128)S(1)} %broadcast_maximum_fusion.1, pred[64,1024]{1,0:T(8,128)(4,1)S(1)} %broadcast_compare_fusion.1), kind=kOutput, calls=%fused_computation.20 | convolution fusion | flops 1612709888 | bytes 6883328 | tf_op jit(solution)/shard_map/cond/branch_1_fun/hmqk,khd->hmqd/dot_general | solution.py:34
  141.6 0.7 fusion.17
  142.3 8.0 %conditional.2 = (f32[4,2,64]{2,1,0:T(2,128)S(1)}, f32[4,2,64,256]{3,2,1,0:T(8,128)S(1)}) conditional(s32[]{:T(128)} %bitcast.2, () %tuple.24, (s32[1024]{0:T(1024)S(1)}, s32[64]{0:T(128)S(1)}, bf16[128,1024]{1,0:T(8,128)(2,1)S(1)}, bf16[1024,4,2,128]{0,3,2,1:T(8,128)(2,1)S(1)}, f32[1024,4,256]{0,2,1:T(8,128)}) %tuple.56), branch_computations={%region_0.0_spmd, %region_1.4_spmd} | conditional | flops 1751186944 | bytes 30818604 | solution.py:90
  142.6 0.7 fusion.2
  143.3 1.5 copy-done.1
  144.7 4.8 %fusion = f32[4,2,64,256]{3,2,1,0:T(8,128)S(1)} fusion(f32[1024,4,256]{0,2,1:T(8,128)S(1)} %copy-done.1, f32[4,2,64,1024]{3,2,1,0:T(8,128)S(1)} %get-tuple-element.61, f32[4,2,64]{2,1,0:T(2,128)S(1)} %broadcast_maximum_fusion, pred[64,1024]{1,0:T(8,128)(4,1)S(1)} %broadcast_compare_fusion), kind=kOutput, calls=%fused_computation.2 | convolution fusion | flops 1612709888 | bytes 6883328 | tf_op jit(solution)/shard_map/cond/branch_1_fun/hmqk,khd->hmqd/dot_general | solution.py:34
  149.6 0.7 fusion.3
  150.3 5.7 %reduce-scatter.2.cloned.1.call-done = bf16[1024,256]{0,1:T(8,128)(2,1)} async-done(((bf16[4096,256]{0,1:T(8,128)(2,1)}), bf16[1024,256]{0,1:T(8,128)(2,1)}) %reduce-scatter.2.cloned.1.call-update) | async-done | bytes 524304 | tf_op jit(solution)/shard_map/reduce_scatter | solution.py:138
  156.0 5.5 %all-to-all-start.1 = ((bf16[1024,8,32]{0,2,1:T(8,128)(2,1)}), bf16[1024,8,32]{0,2,1:T(8,128)(2,1)S(1)}, u32[]{:S(2)}, u32[]{:S(2)}) async-start(bf16[1024,8,32]{0,2,1:T(8,128)(2,1)} %bitcast.102), calls=%async_computation.2 | async-start | bytes 1048576 | tf_op jit(solution)/shard_map/all_to_all | solution.py:146
  161.5 0.3 multiply_reduce_fusion.1
  162.1 0.7 pad_maximum_fusion.1
  162.8 13.0 %all-to-all-done.1 = bf16[1024,8,32]{0,2,1:T(8,128)(2,1)S(1)} async-done(((bf16[1024,8,32]{0,2,1:T(8,128)(2,1)}), bf16[1024,8,32]{0,2,1:T(8,128)(2,1)S(1)}, u32[]{:S(2)}, u32[]{:S(2)}) %all-to-all-start.1) | async-done | bytes 524320 | tf_op jit(solution)/shard_map/all_to_all | solution.py:146
  175.8 0.2 convolution_multiply_fusion.1
  176.0 0.9 fusion.41
  (61 shorter events, 2.1 us)
Async XLA Ops:
  8.0 3.3 %copy-start.8 = (s32[64,2]{0,1:T(2,128)S(1)}, s32[64,2]{0,1:T(2,128)}, u32[]{:S(2)}) copy-start(s32[64,2]{0,1:T(2,128)} %param.23) | copy-start | bytes 1540
  8.0 5.5 %copy-start.3 = (bf16[64,4096]{1,0:T(8,128)(2,1)S(1)}, bf16[64,4096]{1,0:T(8,128)(2,1)}, u32[]{:S(2)}) copy-start(bf16[64,4096]{1,0:T(8,128)(2,1)} %param.21) | copy-start | bytes 1572868
  8.0 5.7 %copy-start.5 = (f32[4096]{0:T(1024)S(1)}, f32[4096]{0:T(1024)}, u32[]{:S(2)}) copy-start(f32[4096]{0:T(1024)} %param.22) | copy-start | bytes 49156
  8.0 120.9 %all-gather.2.cloned.1.call-start = ((), (), s32[]{:S(2)}) async-start(), calls=%async_computation.3 | async-start | bytes 4718592 | tf_op jit(solution)/shard_map/all_gather | solution.py:77
  11.3 144.7 %reduce-scatter.2.cloned.1.call-start = ((), (), s32[]{:S(2)}) async-start(), calls=%async_computation.4 | async-start | bytes 2621440 | tf_op jit(solution)/shard_map/reduce_scatter | solution.py:138
  15.8 101.2 %copy-start.10 = (bf16[1,4096,512]{2,1,0:T(8,128)(2,1)S(1)}, bf16[1,4096,512]{2,1,0:T(8,128)(2,1)}, u32[]{:S(2)}) copy-start(bf16[1,4096,512]{2,1,0:T(8,128)(2,1)} %param.25) | copy-start | bytes 12582916
  115.7 1.3 copy-start.2
  126.1 2.5 %copy-start.6 = (f32[64,2]{0,1:T(2,128)S(1)}, f32[64,2]{0,1:T(2,128)}, u32[]{:S(2)}) copy-start(f32[64,2]{0,1:T(2,128)} %param.24) | copy-start | bytes 1540
  132.0 2.4 %copy-start.4 = (bf16[128,1024]{1,0:T(8,128)(2,1)S(1)}, bf16[128,1024]{1,0:T(8,128)(2,1)}, u32[]{:S(2)}) copy-start(bf16[128,1024]{1,0:T(8,128)(2,1)} %param.16) | copy-start | bytes 786436
  134.6 2.2 %copy-start = (f32[1024,4,256]{0,2,1:T(8,128)S(1)}, f32[1024,4,256]{0,2,1:T(8,128)}, u32[]{:S(2)}) copy-start(f32[1024,4,256]{0,2,1:T(8,128)} %get-tuple-element.53) | copy-start | bytes 12582916 | tf_op jit(solution)/shard_map/cond
  142.3 19.2 %copy-start.9 = (f32[4]{0:T(128)S(1)}, f32[4]{0:T(128)}, u32[]{:S(2)}) copy-start(f32[4]{0:T(128)} %param.19) | copy-start | bytes 52
  142.6 2.2 %copy-start.1 = (f32[1024,4,256]{0,2,1:T(8,128)S(1)}, f32[1024,4,256]{0,2,1:T(8,128)}, u32[]{:S(2)}) copy-start(f32[1024,4,256]{0,2,1:T(8,128)} %get-tuple-element.48) | copy-start | bytes 12582916 | tf_op jit(solution)/shard_map/cond
  150.3 11.6 %copy-start.7 = (f32[256]{0:T(256)S(1)}, f32[256]{0:T(256)}, u32[]{:S(2)}) copy-start(f32[256]{0:T(256)} %param.20) | copy-start | bytes 3076
  156.0 19.8 %all-to-all-start.1 = ((bf16[1024,8,32]{0,2,1:T(8,128)(2,1)}), bf16[1024,8,32]{0,2,1:T(8,128)(2,1)S(1)}, u32[]{:S(2)}, u32[]{:S(2)}) async-start(bf16[1024,8,32]{0,2,1:T(8,128)(2,1)} %bitcast.102), calls=%async_computation.2 | async-start | bytes 1048576 | tf_op jit(solution)/shard_map/all_to_all | solution.py:146
Sparse Core Ops, SparseCore 0:
  11.4 111.2 all-gather.1
Sparse Core Ops, SparseCore 1:
  126.2 29.7 reduce-scatter.1
